TPU v7x, 32 devices: a whole 2x2x4 slice. The times are simulated.
32 devices in a mesh: sp: 8 (over z, y), tp: 4 (over x, core).
Axes of the slice: x: 2, y: 2, z: 4, core: 2. Of those that a mesh axis runs over, the one named last changes fastest.
Arguments:
- residual: bfloat16 [8192, 2048], P('sp'), may hold values from -8 to 8
- query_wide: bfloat16 [8192, 1024], P('sp', 'tp'), may hold values from -6 to 6
- key_wide: bfloat16 [8192, 1024], P('sp', 'tp'), may hold values from -6 to 6
- value_wide: bfloat16 [8192, 2048], P('sp', 'tp'), may hold values from -6 to 6
- decay_wide: bfloat16 [8192, 1024], P('sp', 'tp'), may hold values from -12 to 12
- gate_wide: bfloat16 [8192, 2048], P('sp', 'tp'), may hold values from -6 to 6
- query_narrow: bfloat16 [8192, 512], P('sp', 'tp'), may hold values from -6 to 6
- key_narrow: bfloat16 [8192, 512], P('sp', 'tp'), may hold values from -6 to 6
- value_narrow: bfloat16 [8192, 2048], P('sp', 'tp'), may hold values from -6 to 6
- decay_narrow: bfloat16 [8192, 512], P('sp', 'tp'), may hold values from -12 to 12
- gate_narrow: bfloat16 [8192, 2048], P('sp', 'tp'), may hold values from -6 to 6
- head_gain: float32 [512], replicated, may hold values from 0.1 to 1.9
- out_wide: bfloat16 [2048, 2048], P('tp'), may hold values from -0.125 to 0.125
- out_narrow: bfloat16 [2048, 2048], P('tp'), may hold values from -0.125 to 0.125
- mlp_gain: float32 [2048], replicated, may hold values from 0.1 to 1.9
- up_weight: bfloat16 [2048, 4096], P('sp', 'tp'), may hold values from -0.125 to 0.125
- down_weight: bfloat16 [4096, 2048], P('tp', 'sp'), may hold values from -0.09375 to 0.09375
Outputs:
- layer_out: bfloat16 [8192, 2048], P('sp', 'tp')
All inputs are finite; a program needn't handle non-finite values.
Results may differ from a plain program's by a relative error of at most 0.017.
Values may be sent and summed in bfloat16 or wider, within the bound.
A program may use at most 128 MiB of HBM per device.

v0:
```python
import functools
import jax
import jax.numpy as jnp
from jax import lax
from jax.experimental import pallas as pl
from jax.experimental.pallas import tpu as pltpu
from jax.sharding import PartitionSpec as P

HEADS = 4
EPS = 1e-05
DECAY_NORMALIZER = 16.0
MESH = pl.DeviceIdType.MESH
BF = jnp.bfloat16
F32 = jnp.float32
VM = pltpu.VMEM


def vmem():
    return pl.BlockSpec(memory_space=VM)


def dot(a, b, dims):
    return lax.dot_general(a, b, (dims, ((), ())), preferred_element_type=F32)


NT = ((1,), (1,))
NN = ((1,), (0,))
TN = ((0,), (0,))


def local_group(q, k, v, d, out, carried, memory, offset, tril, scale):
    rows = q.shape[0]
    decay = d[...].astype(F32)
    g = (jnp.minimum(decay, 0.0) - jnp.log1p(jnp.exp(-jnp.abs(decay)))) / DECAY_NORMALIZER
    high = g.astype(BF)
    low = (g - high.astype(F32)).astype(BF)
    ones = tril.astype(F32).astype(BF)
    within = dot(ones, high, NN) + dot(ones, low, NN)
    mid = within[rows // 2 - 1 : rows // 2]
    last = within[rows - 1 : rows]
    scaled_q = q[...].astype(F32) * scale * jnp.exp(within - mid)
    scaled_k = k[...].astype(F32) * jnp.exp(mid - within)
    value = v[...]
    scores = dot(scaled_q.astype(BF), scaled_k.astype(BF), NT)
    scores = jnp.where(tril, scores, 0.0).astype(BF)
    whole_q = scaled_q * jnp.exp(mid)
    state = memory[...]
    out[...] = (dot(scores, value, NN) + dot(whole_q.astype(BF), state.astype(BF), NT)).astype(
        out.dtype
    )
    carried[...] = (whole_q * jnp.exp(offset[...])).astype(BF)
    keys = (scaled_k * jnp.exp(last - mid)).astype(BF)
    memory[...] = state * jnp.exp(last) + dot(value, keys, TN)
    offset[...] = offset[...] + last


def local_kernel(
    qw, kw, vw, dw, qn, kn, vn, dn, ow, cw, on, cn, packed, mw, mn, fw, fn
):
    step = pl.program_id(0)
    rows = qw.shape[0]

    @pl.when(step == 0)
    def _():
        for ref in (mw, mn, fw, fn):
            ref[...] = jnp.zeros_like(ref)

    tril = lax.broadcasted_iota(jnp.int32, (rows, rows), 0) >= lax.broadcasted_iota(
        jnp.int32, (rows, rows), 1
    )
    local_group(qw, kw, vw, dw, ow, cw, mw, fw, tril, qw.shape[1] ** -0.5)
    local_group(qn, kn, vn, dn, on, cn, mn, fn, tril, qn.shape[1] ** -0.5)

    @pl.when(step == pl.num_programs(0) - 1)
    def _():
        wide, values = qw.shape[1], vw.shape[1]
        packed[:values, :wide] = mw[...].astype(BF)
        packed[:values, wide:] = mn[...].astype(BF)
        extra = packed.shape[0] - values
        packed[values:, :wide] = jnp.broadcast_to(jnp.exp(fw[...]), (extra, wide)).astype(BF)
        packed[values:, wide:] = jnp.broadcast_to(
            jnp.exp(fn[...]), (extra, qn.shape[1])
        ).astype(BF)


def local_pass(qw, kw, vw, dw, qn, kn, vn, dn):
    tokens, wide = qw.shape
    narrow, values = qn.shape[1], vw.shape[1]
    rows = min(128, tokens)

    def spec(width):
        return pl.BlockSpec((rows, width), lambda i: (i, 0))

    whole = (values + 16, wide + narrow)
    return pl.pallas_call(
        local_kernel,
        grid=(tokens // rows,),
        in_specs=[spec(x.shape[1]) for x in (qw, kw, vw, dw, qn, kn, vn, dn)],
        out_specs=[
            spec(values), spec(wide), spec(values), spec(narrow),
            pl.BlockSpec(whole, lambda i: (0, 0)),
        ],
        out_shape=[
            jax.ShapeDtypeStruct((tokens, values), BF),
            jax.ShapeDtypeStruct((tokens, wide), BF),
            jax.ShapeDtypeStruct((tokens, values), BF),
            jax.ShapeDtypeStruct((tokens, narrow), BF),
            jax.ShapeDtypeStruct(whole, BF),
        ],
        scratch_shapes=[
            VM((values, wide), F32), VM((values, narrow), F32),
            VM((1, wide), F32), VM((1, narrow), F32),
        ],
        cost_estimate=pl.CostEstimate(
            flops=30 * 10**9, bytes_accessed=12 * 2**20, transcendentals=0
        ),
        name="local_pass",
    )(qw, kw, vw, dw, qn, kn, vn, dn)


def ring_place(n):
    s = lax.axis_index("sp")
    half = n // 2

    def index_of(p):
        p = lax.rem(p + n, n)
        return jnp.where(p < half, 2 * p, 2 * (n - 1 - p) + 1)

    place = jnp.where(lax.rem(s, 2) == 0, s // 2, n - (s + 1) // 2)
    return place, index_of, (index_of(place + 1), index_of(place - 1))


def ring_steps(n, mine, every, send_sem, recv_sem):
    half = n // 2
    place, index_of, sides = ring_place(n)
    cut = mine.shape[0] // 32 * 16
    pieces = (pl.ds(0, cut), pl.ds(cut, mine.shape[0] - cut))
    copies = {}

    def hop(far, piece, way):
        origin = index_of(place - (far - 1) if way == 0 else place + (far - 1))
        if far > 1:
            copies[far - 1, piece, way].wait_recv()
            source = every.at[origin, pieces[piece]]
        else:
            source = mine.at[pieces[piece]]
        copy = pltpu.make_async_remote_copy(
            src_ref=source,
            dst_ref=every.at[origin, pieces[piece]],
            send_sem=send_sem.at[way, far - 1, piece],
            recv_sem=recv_sem.at[way, far - 1, piece],
            device_id={"sp": sides[way]},
            device_id_type=MESH,
        )
        copy.start()
        copies[far, piece, way] = copy

    def close():
        for (far, piece, way), copy in copies.items():
            copy.wait_send()
            if far == half or (far == half - 1 and piece != way):
                copy.wait_recv()

    hops = [
        functools.partial(hop, far, piece, way)
        for far in range(1, half + 1)
        for piece in (0, 1)
        for way in (0, 1)
        if far < half or piece == way
    ]
    return hops, close


def ring_kernel(n, mine, every, send_sem, recv_sem):
    barrier = pltpu.get_barrier_semaphore()
    for side in ring_place(n)[2]:
        pl.semaphore_signal(barrier, inc=1, device_id={"sp": side}, device_id_type=MESH)
    pl.semaphore_wait(barrier, 2)
    hops, close = ring_steps(n, mine, every, send_sem, recv_sem)
    for hop in hops:
        hop()
    every[lax.axis_index("sp")] = mine[...]
    close()


def ring(packed, n):
    return pl.pallas_call(
        functools.partial(ring_kernel, n),
        out_shape=jax.ShapeDtypeStruct((n,) + packed.shape, BF),
        in_specs=[vmem()],
        out_specs=vmem(),
        scratch_shapes=[
            pltpu.SemaphoreType.DMA((2, n // 2, 2)),
            pltpu.SemaphoreType.DMA((2, n // 2, 2)),
        ],
        compiler_params=pltpu.CompilerParams(collective_id=0, has_side_effects=True),
        cost_estimate=pl.CostEstimate(
            flops=30 * 10**9, bytes_accessed=2**20, transcendentals=0
        ),
        name="state_ring",
    )(packed)


def gated(local, carried, state, gate, gain):
    out = local[...].astype(F32) + dot(carried[...], state, NT)
    scale = lax.rsqrt(jnp.mean(jnp.square(out), axis=-1, keepdims=True) + EPS)
    u = gate[...].astype(F32)
    return (out * scale * gain[...] * (u / (1.0 + jnp.exp(-u)))).astype(BF)


def finish_kernel(every, ow, cw, gw, on, cn, gn, gain, weight_w, weight_n, out, total, state):
    wide = cw.shape[1]
    values = ow.shape[1]

    @pl.when(pl.program_id(0) == 0)
    def _():
        total[...] = jnp.zeros_like(total)

        def one(j, carry):
            decay = every[j, values : values + 16, :].astype(F32)[:1]
            total[...] = total[...] * decay + every[j, :values, :].astype(F32)
            return carry

        lax.fori_loop(0, lax.axis_index("sp"), one, 0)
        state[...] = total[...].astype(BF)

    left = gated(ow, cw, state[:, :wide], gw, gain)
    right = gated(on, cn, state[:, wide:], gn, gain)
    out[...] = (dot(left, weight_w[...], NN) + dot(right, weight_n[...], NN)).astype(BF)


def finish(every, ow, cw, gw, on, cn, gn, gain, weight_w, weight_n):
    tokens, values = ow.shape
    rows = min(256, tokens)
    width = weight_w.shape[1]

    def spec(x):
        return pl.BlockSpec((rows, x.shape[1]), lambda i: (i, 0))

    return pl.pallas_call(
        finish_kernel,
        grid=(tokens // rows,),
        in_specs=[vmem()]
        + [spec(x) for x in (ow, cw, gw, on, cn, gn)]
        + [vmem()] * 3,
        out_specs=pl.BlockSpec((rows, width), lambda i: (i, 0)),
        out_shape=jax.ShapeDtypeStruct((tokens, width), BF),
        scratch_shapes=[
            VM((values, every.shape[2]), F32),
            VM((values, every.shape[2]), BF),
        ],
        compiler_params=pltpu.CompilerParams(vmem_limit_bytes=48 * 2**20),
        cost_estimate=pl.CostEstimate(
            flops=20 * 10**9, bytes_accessed=16 * 2**20, transcendentals=0
        ),
        name="finish",
    )(every, ow, cw, gw, on, cn, gn, gain.reshape(1, -1), weight_w, weight_n)


def remote(src, dst, send, recv, to):
    copy = pltpu.make_async_remote_copy(
        src_ref=src, dst_ref=dst, send_sem=send, recv_sem=recv,
        device_id={"tp": to}, device_id_type=MESH,
    )
    copy.start()
    return copy


def greet(t, sides=()):
    barrier = pltpu.get_barrier_semaphore()
    near, far = t + 1 - 2 * lax.rem(t, 2), lax.rem(t + 2, 4)
    for other in (near, far):
        pl.semaphore_signal(barrier, inc=1, device_id={"tp": other}, device_id_type=MESH)
    for side in sides:
        pl.semaphore_signal(barrier, inc=1, device_id={"sp": side}, device_id_type=MESH)
    pl.semaphore_wait(barrier, 2 + len(sides))
    return near, far, lax.rem(near + 2, 4)


def reduce_steps(block, chunks, t, near, far, cross, partial, r1, mix, r2, sems, use):
    s1, v1, s2, v2 = sems
    rows = mix.shape[1]
    sent = []
    for which, owner in ((1, cross), (0, near)):
        for c in range(chunks):
            sent.append(
                (which, c, remote(
                    partial.at[block(owner, c)], r1.at[which, c],
                    s1.at[which, c], v1.at[which, c], near,
                ))
            )
    first = {(w, c): x for w, c, x in sent}
    second = []
    for c in range(chunks):
        first[1, c].wait_recv()
        mix[c] = (partial[block(far, c)].astype(F32) + r1[1, c].astype(F32)).astype(BF)
        second.append(remote(mix.at[c], r2.at[c], s2.at[c], v2.at[c], far))
    for c in range(chunks):
        first[0, c].wait_recv()
        second[c].wait_recv()
        use(c, partial[block(t, c)].astype(F32) + r1[0, c].astype(F32) + r2[c].astype(F32))
    return [x for _, _, x in sent] + second


def mix_kernel(
    n, chunks, partial, residual, gain, shard, stream, normed, weight,
    r1, mix, r2, s1, v1, s2, v2, sx, vx, sn, vn, sf, vf, sw, vw,
):
    t = lax.axis_index("tp")
    near, far, cross = greet(t, ring_place(n)[2])
    hops, close = ring_steps(n, shard, weight, sw, vw)
    first = [hop for hop in hops if hop.args[0] == 1]
    later = [hop for hop in hops if hop.args[0] > 1]
    for hop in first:
        hop()
    rows = mix.shape[1]
    own = rows * chunks

    def block(owner, c):
        return pl.ds(pl.multiple_of(owner * own + c * rows, rows), rows), slice(None)

    def norm(where):
        x = stream[where].astype(F32)
        scale = lax.rsqrt(jnp.mean(jnp.square(x), axis=1, keepdims=True) + EPS)
        normed[where] = (x * scale * gain[...]).astype(BF)

    across, beside, relayed = [], [], []

    def use(c, value):
        where = block(t, c)
        stream[where] = (residual[pl.ds(c * rows, rows), :].astype(F32) + value).astype(BF)
        across.append(remote(stream.at[where], stream.at[where], sx.at[c], vx.at[c], far))
        beside.append(remote(stream.at[where], stream.at[where], sn.at[c], vn.at[c], near))
        for hop in later[2 * c : 2 * c + 2]:
            hop()

    started = reduce_steps(
        block, chunks, t, near, far, cross, partial, r1, mix, r2, (s1, v1, s2, v2), use
    )
    for c in range(chunks):
        norm(block(t, c))
        beside[c].wait_recv()
        norm(block(near, c))
    weight[lax.axis_index("sp")] = shard[...]
    for hop in later[2 * chunks :]:
        hop()
    for c in range(chunks):
        across[c].wait_recv()
        where = block(far, c)
        relayed.append(remote(stream.at[where], stream.at[where], sf.at[c], vf.at[c], near))
        norm(where)
    for c in range(chunks):
        relayed[c].wait_recv()
        norm(block(cross, c))
    for copy in started + across + beside + relayed:
        copy.wait_send()
    close()


def mix_rows(partial, residual, gain, shard, n):
    tokens, width = partial.shape
    chunks = 4
    rows = tokens // 4 // chunks
    dma = pltpu.SemaphoreType.DMA
    return pl.pallas_call(
        functools.partial(mix_kernel, n, chunks),
        out_shape=[jax.ShapeDtypeStruct((tokens, width), BF)] * 2
        + [jax.ShapeDtypeStruct((n,) + shard.shape, BF)],
        in_specs=[vmem()] * 4,
        out_specs=[vmem()] * 3,
        scratch_shapes=[
            VM((2, chunks, rows, width), BF), VM((chunks, rows, width), BF),
            VM((chunks, rows, width), BF),
            dma((2, chunks)), dma((2, chunks)),
        ] + [dma((chunks,))] * 8 + [dma((2, n // 2, 2))] * 2,
        compiler_params=pltpu.CompilerParams(
            collective_id=1, has_side_effects=True, vmem_limit_bytes=48 * 2**20
        ),
        cost_estimate=pl.CostEstimate(
            flops=50 * 10**9, bytes_accessed=16 * 2**20, transcendentals=0
        ),
        name="mix_rows",
    )(partial, residual, gain.reshape(1, -1), shard)


def mixer_kernel(
    chunks, normed, up, down, stream, out, partial, r1, mix, r2, s1, v1, s2, v2
):
    t = lax.axis_index("tp")
    near, far, cross = greet(t)
    rows, width = mix.shape[1:]

    def line(c):
        return pl.ds(pl.multiple_of(c * rows, rows), rows)

    def block(owner, c):
        return line(c), pl.ds(pl.multiple_of(owner * width, width), width)

    def first(which, c):
        return pltpu.make_async_remote_copy(
            src_ref=partial.at[block((near, cross)[which], c)],
            dst_ref=r1.at[which, c],
            send_sem=s1.at[which, c],
            recv_sem=v1.at[which, c],
            device_id={"tp": near},
            device_id_type=MESH,
        )

    def second(c):
        return pltpu.make_async_remote_copy(
            src_ref=mix.at[c], dst_ref=r2.at[c], send_sem=s2.at[c], recv_sem=v2.at[c],
            device_id={"tp": far}, device_id_type=MESH,
        )

    def across(c):
        first(1, c).wait_recv()
        mix[c] = (partial[block(far, c)].astype(F32) + r1[1, c].astype(F32)).astype(BF)
        second(c).start()

    def step(c, carry):
        hidden = jnp.square(jnp.maximum(dot(normed[line(c), :], up[...], NN), 0.0)).astype(BF)
        partial[line(c), :] = dot(hidden, down[...], NN).astype(BF)
        first(1, c).start()
        first(0, c).start()

        @pl.when(c > 0)
        def _():
            across(c - 1)

        return carry

    lax.fori_loop(0, chunks, step, 0)
    across(chunks - 1)

    def close(c, carry):
        first(0, c).wait_recv()
        second(c).wait_recv()
        value = partial[block(t, c)].astype(F32) + r1[0, c].astype(F32) + r2[c].astype(F32)
        out[line(c), :] = (stream[line(c), :].astype(F32) + value).astype(BF)
        first(0, c).wait_send()
        first(1, c).wait_send()
        second(c).wait_send()
        return carry

    lax.fori_loop(0, chunks, close, 0)


def channel_mixer(normed, up, down, stream):
    tokens, width = stream.shape
    chunks = 4
    rows = tokens // chunks
    dma = pltpu.SemaphoreType.DMA
    return pl.pallas_call(
        functools.partial(mixer_kernel, chunks),
        out_shape=jax.ShapeDtypeStruct((tokens, width), BF),
        in_specs=[vmem()] * 4,
        out_specs=vmem(),
        scratch_shapes=[
            VM((tokens, down.shape[1]), BF),
            VM((2, chunks, rows, width), BF), VM((chunks, rows, width), BF),
            VM((chunks, rows, width), BF),
            dma((2, chunks)), dma((2, chunks)), dma((chunks,)), dma((chunks,)),
        ],
        compiler_params=pltpu.CompilerParams(
            collective_id=2, has_side_effects=True, vmem_limit_bytes=56 * 2**20
        ),
        name="channel_mixer",
    )(normed, up, down, stream)


def body(
    residual,
    query_wide,
    key_wide,
    value_wide,
    decay_wide,
    gate_wide,
    query_narrow,
    key_narrow,
    value_narrow,
    decay_narrow,
    gate_narrow,
    head_gain,
    out_wide,
    out_narrow,
    mlp_gain,
    up_weight,
    down_weight,
):
    n_sp, n_tp = lax.axis_size("sp"), lax.axis_size("tp")
    assert n_tp == HEADS == 4 and n_sp % 2 == 0
    down_whole = lax.all_gather(down_weight, "sp", axis=1, tiled=True)
    wide_out, wide_q, narrow_out, narrow_q, packed = local_pass(
        query_wide, key_wide, value_wide, decay_wide,
        query_narrow, key_narrow, value_narrow, decay_narrow,
    )
    every = ring(packed, n_sp)
    partial = finish(
        every, wide_out, wide_q, gate_wide, narrow_out, narrow_q, gate_narrow,
        head_gain, out_wide, out_narrow,
    )
    t = lax.axis_index("tp")
    own_rows = residual.shape[0] // n_tp
    own_cols = residual.shape[1] // n_tp
    residual_rows = lax.dynamic_slice_in_dim(residual, t * own_rows, own_rows, 0)
    stream, normed, up_whole = mix_rows(partial, residual_rows, mlp_gain, up_weight, n_sp)
    up_whole = up_whole.reshape(-1, up_weight.shape[1])
    stream_cols = lax.dynamic_slice_in_dim(stream, t * own_cols, own_cols, 1)
    return channel_mixer(normed, up_whole, down_whole, stream_cols)


def solution(mesh):
    return jax.shard_map(
        body,
        mesh=mesh,
        in_specs=(
            P("sp", None),
            P("sp", "tp"),
            P("sp", "tp"),
            P("sp", "tp"),
            P("sp", "tp"),
            P("sp", "tp"),
            P("sp", "tp"),
            P("sp", "tp"),
            P("sp", "tp"),
            P("sp", "tp"),
            P("sp", "tp"),
            P(),
            P("tp", None),
            P("tp", None),
            P(),
            P("sp", "tp"),
            P("tp", "sp"),
        ),
        out_specs=P("sp", "tp"),
        check_vma=False,
    )
```

profile of v0, /device:TPU:28, one launch (start us, length us, event | category | flops | bytes accessed | tf_op | source)
XLA Modules:
  0.0 201.9 jit_solution(6037882866903326684)
XLA Ops:
  6.5 0.0 all-gather.2.cloned.1.call-start
  6.5 0.7 all-gather.2.cloned.1.call-update
  7.3 10.9 %local_pass.1 = (bf16[1024,512]{1,0:T(8,128)(2,1)}, bf16[1024,256]{1,0:T(8,128)(2,1)}, bf16[1024,512]{1,0:T(8,128)(2,1)}, bf16[1024,128]{1,0:T(8,128)(2,1)}, bf16[528,384]{1,0:T(8,128)(2,1)}) custom-call(bf16[1024,256]{1,0:T(8,128)(2,1)} %qw.1, bf16[1024,256]{1,0:T(8,128)(2,1)} %kw.1, bf16[1024,512]{1,0:T(8,128)(2,1)} %vw.1, bf16[1024,256]{1,0:T(8,128)(2,1)} %dw.1, ...), custom_call_target="tpu_custom_call" | custom-call | flops 30000001024 | bytes 12582912 | tf_op jit(solution)/shard_map/local_pass/pallas_call | solution.py:95
  18.2 0.0 copy-start
  18.2 0.0 copy-start.1
  18.2 0.0 copy-start.4
  18.2 0.0 copy-start.5
  18.2 0.0 copy-start.8
  18.2 64.6 %state_ring.1.every = bf16[8,528,384]{2,1,0:T(8,128)(2,1)} custom-call(bf16[528,384]{1,0:T(8,128)(2,1)} %get-tuple-element.13.mine), custom_call_target="tpu_custom_call" | custom-call | flops 30000001024 | bytes 1048576 | tf_op jit(solution)/shard_map/state_ring/pallas_call | solution.py:187
  82.8 1.3 constant_dynamic-slice_fusion.1.residual
  84.1 0.0 copy-done
  84.2 0.0 copy-done.1
  84.2 0.0 copy-done.4
  84.2 0.0 copy-done.5
  84.2 0.0 copy-done.8
  84.2 0.0 copy-start.6
  84.2 1.2 copy-done.6
  85.4 0.0 copy-start.7
  85.4 1.0 copy-done.7
  86.5 0.0 copy-start.2
  86.5 0.0 copy-start.3
  86.5 11.8 %finish.1.partial = bf16[1024,2048]{1,0:T(8,128)(2,1)} custom-call(bf16[8,528,384]{2,1,0:T(8,128)(2,1)} %state_ring.1.every, bf16[1024,512]{1,0:T(8,128)(2,1)S(1)} %copy-done.5, bf16[1024,256]{1,0:T(8,128)(2,1)S(1)} %copy-done.7, bf16[1024,512]{1,0:T(8,128)(2,1)S(1)} %copy-done, bf16[1024,512]{1,0:T(8,128)(2,1)S(1)} %copy-done.6, ...), custom_call_target="tpu_custom_call" | custom-call | flops 20000000000 | bytes 16777216 | tf_op jit(solution)/shard_map/finish/pallas_call | solution.py:240
  98.3 0.0 copy-done.2
  98.3 0.0 copy-done.3
  98.3 56.8 %mix_rows.1 = (bf16[1024,2048]{1,0:T(8,128)(2,1)S(1)}, bf16[1024,2048]{1,0:T(8,128)(2,1)}, bf16[8,256,1024]{2,1,0:T(8,128)(2,1)}) custom-call(bf16[1024,2048]{1,0:T(8,128)(2,1)} %finish.1.partial, bf16[256,2048]{1,0:T(8,128)(2,1)S(1)} %constant_dynamic-slice_fusion.1.residual, f32[1,2048]{1,0:T(1,128)S(1)} %bitcast.3, bf16[256,1024]{1,0:T(8,128)(2,1)S(1)} %copy-done.2), custom_call_target="tpu_custom_call" | custom-call | flops 49999998976 | bytes 16777216 | tf_op jit(solution)/shard_map/mix_rows/pallas_call | solution.py:365
  155.1 1.1 constant_dynamic-slice_fusion.stream
  156.2 0.0 all-gather.2.cloned.1.call-done.down
  156.2 36.6 %channel_mixer.1 = bf16[1024,512]{1,0:T(8,128)(2,1)} custom-call(bf16[1024,2048]{1,0:T(8,128)(2,1)} %get-tuple-element.18.normed, bf16[2048,1024]{1,0:T(8,128)(2,1)} %bitcast.5, bf16[1024,2048]{1,0:T(8,128)(2,1)} %all-gather.2.cloned.1.call-done.down, bf16[1024,512]{1,0:T(8,128)(2,1)} %constant_dynamic-slice_fusion.stream), custom_call_target="tpu_custom_call" | custom-call | tf_op jit(solution)/shard_map/channel_mixer/pallas_call | solution.py:453
  192.8 2.3 %copy.19 = bf16[1024,512]{1,0:T(8,128)(2,1)} copy(bf16[1024,512]{1,0:T(8,128)(2,1)} %channel_mixer.1) | data formatting | bytes 2097152
Async XLA Ops:
  6.5 149.7 %all-gather.2.cloned.1.call-start = ((), (), s32[]{:S(2)}) async-start(), calls=%async_computation | async-start | bytes 4718592 | tf_op jit(solution)/shard_map/all_gather | solution.py:492
  18.2 66.0 %copy-start = (bf16[1024,512]{1,0:T(8,128)(2,1)S(1)}, bf16[1024,512]{1,0:T(8,128)(2,1)}, u32[]{:S(2)}) copy-start(bf16[1024,512]{1,0:T(8,128)(2,1)} %gw.1) | copy-start | bytes 3145732
  18.2 66.0 %copy-start.1 = (bf16[1024,512]{1,0:T(8,128)(2,1)S(1)}, bf16[1024,512]{1,0:T(8,128)(2,1)}, u32[]{:S(2)}) copy-start(bf16[1024,512]{1,0:T(8,128)(2,1)} %gn.1) | copy-start | bytes 3145732
  18.2 66.0 %copy-start.4 = (f32[512]{0:T(512)S(1)}, f32[512]{0:T(512)}, u32[]{:S(2)}) copy-start(f32[512]{0:T(512)} %param.28) | copy-start | bytes 6148
  18.2 66.0 %copy-start.5 = (bf16[1024,512]{1,0:T(8,128)(2,1)S(1)}, bf16[1024,512]{1,0:T(8,128)(2,1)}, u32[]{:S(2)}) copy-start(bf16[1024,512]{1,0:T(8,128)(2,1)} %get-tuple-element.14.ow) | copy-start | bytes 3145732
  18.2 66.0 %copy-start.8 = (bf16[1024,128]{1,0:T(8,128)(2,1)S(1)}, bf16[1024,128]{1,0:T(8,128)(2,1)}, u32[]{:S(2)}) copy-start(bf16[1024,128]{1,0:T(8,128)(2,1)} %get-tuple-element.17.cn) | copy-start | bytes 786436
  84.2 1.2 copy-start.6
  85.4 1.0 copy-start.7
  86.5 11.8 %copy-start.2 = (bf16[256,1024]{1,0:T(8,128)(2,1)S(1)}, bf16[256,1024]{1,0:T(8,128)(2,1)}, u32[]{:S(2)}) copy-start(bf16[256,1024]{1,0:T(8,128)(2,1)} %shard.1) | copy-start | bytes 1572868
  86.5 11.8 %copy-start.3 = (f32[2048]{0:T(1024)S(1)}, f32[2048]{0:T(1024)}, u32[]{:S(2)}) copy-start(f32[2048]{0:T(1024)} %param.31) | copy-start | bytes 24580
Sparse Core Ops, SparseCore 0:
  9.4 93.7 all-gather.1
where the time goes:
time: 204 us; the launch traced here: 202 us
  Pallas kernels  181 us (89%)
  between operations  13.5 us (7%)
  local copies, waits for them, and re-layouts  6.99 us (3%)
    pallas_call x1, Pallas kernels, ring(): pl.pallas_call(functools.partial(ring_kernel, n), out_shape=jax.ShapeDtyp...  64.6 us
    pallas_call x1, Pallas kernels, mix_rows(): pl.pallas_call(functools.partial(mix_kernel, n, chunks), out_shape=[jax.S...  56.8 us
    pallas_call x1, Pallas kernels, channel_mixer(): pl.pallas_call(functools.partial(mixer_kernel, chunks), out_shape=jax.Sha...  36.6 us
    pallas_call x1, Pallas kernels, finish(): pl.pallas_call(finish_kernel, grid=(tokens // rows,), in_specs=[vmem()] +...  11.8 us
    pallas_call x1, Pallas kernels, local_pass(): pl.pallas_call(local_kernel, grid=(tokens // rows,), in_specs=[spec(x.sha...  10.9 us
    unnamed x19, local copies, waits for them, and re-layouts  4.56 us
  transfers between devices with their start and end apart: 1, of which 0 were waited for; matrix products, arithmetic and copies ran while one was open for 1% of the time, Pallas kernels for 71%

commit v1 on v0

v1 whole, which is shorter than its diff:
```python
import functools
import jax
import jax.numpy as jnp
from jax import lax
from jax.experimental import pallas as pl
from jax.experimental.pallas import tpu as pltpu
from jax.sharding import PartitionSpec as P

HEADS = 4
EPS = 1e-05
DECAY_NORMALIZER = 16.0
MESH = pl.DeviceIdType.MESH
BF = jnp.bfloat16
F32 = jnp.float32
VM = pltpu.VMEM
DMA = pltpu.SemaphoreType.DMA
SCAN_CHUNKS = 2
ROW_CHUNKS = 4

NT = ((1,), (1,))
NN = ((1,), (0,))
TN = ((0,), (0,))


def dot(a, b, dims):
    return lax.dot_general(a, b, (dims, ((), ())), preferred_element_type=F32)


def span(i, size):
    return pl.ds(pl.multiple_of(i * size, size), size)


def layer_kernel(
    n,
    residual, qw, kw, vw, dw, gw, qn, kn, vn, dn, gn, gain, outw, outn, mgain, up, down,
    out,
    q_all, k_all, d_all, v_wide, v_narrow, g_wide, g_narrow, w_out, res, d_shard, weights,
    within_all, keys_all, snaps, offsets, total, state, local_w, local_n, carried,
    e1s, e1r, chain_s, chain_r, e2s, prefix,
    gated, partial, near_r, pair_s, cross_r, stream, normed, hidden,
    r1, mix, r2,
    load, ring_s, ring_v, e1_s, e1_v, ch_s, ch_v, e2_s, e2_v,
    na_s, na_v, cr_s, cr_v, st_s, st_v, s1, v1, s2, v2,
):
    s, t = lax.axis_index("sp"), lax.axis_index("tp")
    z, y = s // 2, lax.rem(s, 2)
    m, half_ring = n // 2, n // 2
    u = lax.rem(t, 2)
    near, far = t + 1 - 2 * u, lax.rem(t + 2, 4)
    cross = lax.rem(near + 2, 4)
    tokens, wide = qw.shape
    keys = wide + qn.shape[1]
    values = vw.shape[1]
    groups = ((0, wide, v_wide, local_w), (wide, keys, v_narrow, local_n))

    rows_chunk = tokens // ROW_CHUNKS
    half_rows = rows_chunk // 2
    shard_rows = up.shape[0]
    pairs = [
        (up, weights.at[0, span(s, shard_rows)]),
        (dw, d_all.at[:, :wide]), (dn, d_all.at[:, wide:]),
        (kw, k_all.at[:, :wide]), (kn, k_all.at[:, wide:]),
        (vw, v_wide), (vn, v_narrow),
        (down, d_shard),
        (qw, q_all.at[:, :wide]), (qn, q_all.at[:, wide:]),
        (gw, g_wide), (gn, g_narrow),
        (outw, w_out.at[:values]), (outn, w_out.at[values:]),
    ] + [
        (residual.at[pl.ds(pl.multiple_of(c * rows_chunk + u * half_rows, half_rows), half_rows)],
         res.at[c])
        for c in range(ROW_CHUNKS)
    ]
    loads = [
        pltpu.make_async_copy(a, b, load.at[i]) for i, (a, b) in enumerate(pairs)
    ]
    for copy in loads:
        copy.start()

    place = jnp.where(y == 0, z, n - 1 - z)

    def index_of(p):
        p = lax.rem(p + 2 * n, n)
        return jnp.where(p < m, 2 * p, 2 * (n - 1 - p) + 1)

    barrier = pltpu.get_barrier_semaphore()
    partner = s + 1 - 2 * y
    for other in (index_of(place + 1), index_of(place - 1), partner):
        pl.semaphore_signal(barrier, inc=1, device_id={"sp": other}, device_id_type=MESH)
    for other in (near, far):
        pl.semaphore_signal(barrier, inc=1, device_id={"tp": other}, device_id_type=MESH)
    pl.semaphore_wait(barrier, 5)

    cut = shard_rows // 2

    def hop_copy(kind, dist, first, side):
        way = lax.rem(side + y, 2)
        step = 1 - 2 * way
        piece = way if first else 1 - way
        origin = index_of(place - step * (dist - 1))
        rows = pl.ds(pl.multiple_of(origin * shard_rows + piece * cut, cut), cut)
        return pltpu.make_async_remote_copy(
            src_ref=weights.at[kind, rows], dst_ref=weights.at[kind, rows],
            send_sem=ring_s.at[kind, way, dist - 1, piece],
            recv_sem=ring_v.at[kind, way, dist - 1, piece],
            device_id={"sp": index_of(place + step)}, device_id_type=MESH,
        )

    def hop(kind, dist, first, side):
        if dist > 1:
            hop_copy(kind, dist - 1, first, side).wait_recv()
        hop_copy(kind, dist, first, side).start()

    def hops(kind, dist):
        for first in (True, False) if dist < half_ring else (True,):
            for side in (0, 1):
                hop(kind, dist, first, side)

    def arrive(kind):
        for side in (0, 1):
            hop_copy(kind, half_ring, True, side).wait_recv()
            if half_ring > 1:
                hop_copy(kind, half_ring - 1, False, side).wait_recv()

    loads[0].wait()
    hop(0, 1, True, 0)
    hop(0, 1, True, 1)

    block = min(128, tokens)
    blocks = tokens // block
    tril = lax.broadcasted_iota(jnp.int32, (block, block), 0) >= lax.broadcasted_iota(
        jnp.int32, (block, block), 1
    )
    ones = tril.astype(F32).astype(BF)
    total[...] = jnp.zeros_like(total)
    state[...] = jnp.zeros_like(state)
    for copy in loads[1:7]:
        copy.wait()

    def pass_one(i, carry):
        rows = span(i, block)
        decay = d_all[rows, :].astype(F32)
        g = (jnp.minimum(decay, 0.0) - jnp.log1p(jnp.exp(-jnp.abs(decay)))) / DECAY_NORMALIZER
        high = g.astype(BF)
        low = (g - high.astype(F32)).astype(BF)
        within = dot(ones, high, NN) + dot(ones, low, NN)
        within_all[rows, :] = within
        mid = within[block // 2 - 1 : block // 2]
        last = within[block - 1 : block]
        scaled = k_all[rows, :].astype(F32) * jnp.exp(mid - within)
        keys_all[rows, :] = scaled.astype(BF)
        ends = (scaled * jnp.exp(last - mid)).astype(BF)
        fade = jnp.exp(last)
        for lo, hi, v, _ in groups:
            before = state[:, lo:hi]
            snaps[i, :, lo:hi] = before.astype(BF)
            state[:, lo:hi] = before * fade[:, lo:hi] + dot(v[rows, :], ends[:, lo:hi], TN)
        offsets[i] = total[...]
        total[...] = total[...] + last
        return carry

    lax.fori_loop(0, blocks, pass_one, 0)

    half = values // 2
    part = half // SCAN_CHUNKS
    mine = jnp.exp(total[...])
    mine_high = mine.astype(BF)
    mine_low = (mine - mine_high.astype(F32)).astype(BF)
    e1s[:8, :] = jnp.broadcast_to(mine_high.astype(F32), (8, keys)).astype(BF)
    e1s[8:16, :] = jnp.broadcast_to(mine_low.astype(F32), (8, keys)).astype(BF)
    e1s[16:, :] = state[span(1 - y, half), :].astype(BF)

    def e1_copy(c):
        where = pl.ds(0, 16 + part) if c == 0 else pl.ds(16 + c * part, part)
        return pltpu.make_async_remote_copy(
            src_ref=e1s.at[where], dst_ref=e1r.at[where], send_sem=e1_s.at[c],
            recv_sem=e1_v.at[c], device_id={"sp": partner}, device_id_type=MESH,
        )

    def chain_copy(c):
        where = pl.ds(c * part, part)
        return pltpu.make_async_remote_copy(
            src_ref=chain_s.at[where], dst_ref=chain_r.at[where], send_sem=ch_s.at[c],
            recv_sem=ch_v.at[c], device_id={"sp": lax.rem(s + 2, n)}, device_id_type=MESH,
        )

    def e2_copy(c):
        return pltpu.make_async_remote_copy(
            src_ref=e2s.at[pl.ds(c * part, part)],
            dst_ref=prefix.at[pl.ds(pl.multiple_of(y * half + c * part, part), part)],
            send_sem=e2_s.at[c], recv_sem=e2_v.at[c], device_id={"sp": partner},
            device_id_type=MESH,
        )

    for c in range(SCAN_CHUNKS):
        e1_copy(c).start()

    hop(0, 1, False, 1)
    hop(0, 1, False, 0)
    loads[7].wait()
    weights[1, span(s, shard_rows), :] = d_shard[...].T
    hop(1, 1, True, 1)
    hop(1, 1, False, 1)
    early_a = z >= 1
    early_b = jnp.logical_and(z >= 2, z < m - 1)

    @pl.when(early_a)
    def _():
        hop(1, 1, True, 0)

    @pl.when(early_b)
    def _():
        hop(1, 1, False, 0)

    for copy in loads[8:10]:
        copy.wait()
    column = lax.broadcasted_iota(jnp.int32, (1, keys), 1)
    scale = jnp.where(column < wide, wide ** -0.5, (keys - wide) ** -0.5).astype(F32)

    def pass_two(i, carry):
        rows = span(i, block)
        within = within_all[rows, :]
        mid = within[block // 2 - 1 : block // 2]
        scaled = q_all[rows, :].astype(F32) * scale * jnp.exp(within - mid)
        whole = scaled * jnp.exp(mid)
        scaled = scaled.astype(BF)
        carried[rows, :] = (whole * jnp.exp(offsets[i])).astype(BF)
        whole = whole.astype(BF)
        for lo, hi, v, local in groups:
            scores = dot(scaled[:, lo:hi], keys_all[rows, lo:hi], NT)
            scores = jnp.where(tril, scores, 0.0).astype(BF)
            local[rows, :] = (
                dot(scores, v[rows, :], NN) + dot(whole[:, lo:hi], snaps[i, :, lo:hi], NT)
            ).astype(BF)
        return carry

    ahead = jnp.minimum(z * (blocks // 2), blocks)
    lax.fori_loop(0, ahead, pass_two, 0)

    @pl.when(z == 0)
    def _():
        chain_r[...] = jnp.zeros_like(chain_r)

    for c in range(SCAN_CHUNKS):
        e1_copy(c).wait_recv()

        @pl.when(z > 0)
        def _():
            chain_copy(c).wait_recv()

        other = e1r[:8, :].astype(F32)[:1] + e1r[8:16, :].astype(F32)[:1]
        fade_even = jnp.where(y == 0, mine, other)
        fade_odd = jnp.where(y == 0, other, mine)
        where = pl.ds(c * part, part)
        own = state[pl.ds(pl.multiple_of(y * half + c * part, part), part), :]
        theirs = e1r[16 + c * part : 16 + (c + 1) * part, :].astype(F32)
        even = jnp.where(y == 0, own, theirs)
        odd = jnp.where(y == 0, theirs, own)
        before = chain_r[where, :].astype(F32)
        between = before * fade_even + even
        chain_s[where, :] = (between * fade_odd + odd).astype(BF)

        @pl.when(z < m - 1)
        def _():
            chain_copy(c).start()

        prefix[pl.ds(pl.multiple_of(y * half + c * part, part), part), :] = jnp.where(
            y == 0, before, between
        ).astype(BF)
        e2s[where, :] = jnp.where(y == 0, between, before).astype(BF)
        e2_copy(c).start()

    @pl.when(jnp.logical_not(early_a))
    def _():
        hop(1, 1, True, 0)

    @pl.when(jnp.logical_not(early_b))
    def _():
        hop(1, 1, False, 0)

    lax.fori_loop(ahead, blocks, pass_two, 0)
    if half_ring >= 2:
        hops(0, 2)
        hops(1, 2)
    for copy in loads[10:]:
        copy.wait()
    for c in range(SCAN_CHUNKS):
        e2_copy(c).wait_recv()

    def near_copy(c):
        return pltpu.make_async_remote_copy(
            src_ref=partial.at[
                pl.ds(pl.multiple_of(c * rows_chunk + (1 - u) * half_rows, half_rows), half_rows)
            ],
            dst_ref=near_r.at[c], send_sem=na_s.at[c], recv_sem=na_v.at[c],
            device_id={"tp": near}, device_id_type=MESH,
        )

    def cross_copy(c):
        return pltpu.make_async_remote_copy(
            src_ref=pair_s.at[c], dst_ref=cross_r.at[c], send_sem=cr_s.at[c],
            recv_sem=cr_v.at[c], device_id={"tp": far}, device_id_type=MESH,
        )

    def own_rows(c):
        return pl.ds(pl.multiple_of(c * rows_chunk + u * half_rows, half_rows), half_rows)

    def other_rows(c):
        return pl.ds(
            pl.multiple_of(c * rows_chunk + (1 - u) * half_rows, half_rows), half_rows
        )

    def stream_copy(c):
        return pltpu.make_async_remote_copy(
            src_ref=stream.at[own_rows(c)], dst_ref=stream.at[own_rows(c)],
            send_sem=st_s.at[c], recv_sem=st_v.at[c],
            device_id={"tp": near}, device_id_type=MESH,
        )

    width = w_out.shape[1]
    tile = min(512, width)

    def project(c, carry):
        rows = span(c, rows_chunk)
        for j, (lo, hi, _, local) in enumerate(groups):
            gate = (g_wide, g_narrow)[j]
            x = local[rows, :].astype(F32) + dot(carried[rows, lo:hi], prefix[:, lo:hi], NT)
            fit = lax.rsqrt(jnp.mean(jnp.square(x), axis=-1, keepdims=True) + EPS)
            v = gate[rows, :].astype(F32)
            gated[:, j * values : (j + 1) * values] = (
                x * fit * gain[...] * (v / (1.0 + jnp.exp(-v)))
            ).astype(BF)
        for lo in range(0, width, tile):
            partial[rows, lo : lo + tile] = dot(
                gated[...], w_out[:, lo : lo + tile], NN
            ).astype(BF)
        near_copy(c).start()

        @pl.when(c > 0)
        def _():
            pair(c - 1)

        return carry

    def pair(c):
        near_copy(c).wait_recv()
        pair_s[c] = (partial[own_rows(c), :].astype(F32) + near_r[c].astype(F32)).astype(BF)
        cross_copy(c).start()

    lax.fori_loop(0, ROW_CHUNKS, project, 0)
    pair(ROW_CHUNKS - 1)

    def norm(rows):
        x = stream[rows, :].astype(F32)
        fit = lax.rsqrt(jnp.mean(jnp.square(x), axis=1, keepdims=True) + EPS)
        normed[rows, :] = (x * fit * mgain[...]).astype(BF)

    def settle(c):
        cross_copy(c).wait_recv()
        value = pair_s[c].astype(F32) + cross_r[c].astype(F32)
        stream[own_rows(c), :] = (res[c].astype(F32) + value).astype(BF)
        stream_copy(c).start()
        norm(own_rows(c))
        stream_copy(c).wait_recv()
        norm(other_rows(c))

    inner = up.shape[1]
    tile_h = min(512, inner)

    def expand(c, carry):
        rows = span(c, rows_chunk)
        for lo in range(0, inner, tile_h):
            h = dot(normed[rows, :], weights[0, :, lo : lo + tile_h], NN)
            hidden[rows, lo : lo + tile_h] = jnp.square(jnp.maximum(h, 0.0)).astype(BF)
        return carry

    for dist in range(3, half_ring):
        hops(0, dist)
    settle(0)
    settle(1)
    if half_ring >= 3:
        hops(0, half_ring)
    for dist in range(3, half_ring):
        hops(1, dist)
    settle(2)
    arrive(0)
    lax.fori_loop(0, 3, expand, 0)
    settle(3)
    if half_ring >= 3:
        hops(1, half_ring)
    expand(3, 0)
    arrive(1)
    for c in range(ROW_CHUNKS):
        near_copy(c).wait_send()

    own_width = out.shape[1]

    def cols(owner):
        return span(owner, own_width)

    def first(which, c):
        return pltpu.make_async_remote_copy(
            src_ref=partial.at[span(c, rows_chunk), cols((near, cross)[which])],
            dst_ref=r1.at[which, c], send_sem=s1.at[which, c], recv_sem=v1.at[which, c],
            device_id={"tp": near}, device_id_type=MESH,
        )

    def second(c):
        return pltpu.make_async_remote_copy(
            src_ref=mix.at[c], dst_ref=r2.at[c], send_sem=s2.at[c], recv_sem=v2.at[c],
            device_id={"tp": far}, device_id_type=MESH,
        )

    def across(c):
        first(1, c).wait_recv()
        rows = span(c, rows_chunk)
        mix[c] = (partial[rows, cols(far)].astype(F32) + r1[1, c].astype(F32)).astype(BF)
        second(c).start()

    def contract(c, carry):
        rows = span(c, rows_chunk)
        for lo in range(0, width, tile):
            partial[rows, lo : lo + tile] = dot(
                hidden[rows, :], weights[1, lo : lo + tile, :], NT
            ).astype(BF)
        first(1, c).start()
        first(0, c).start()

        @pl.when(c > 0)
        def _():
            across(c - 1)

        return carry

    lax.fori_loop(0, ROW_CHUNKS, contract, 0)
    across(ROW_CHUNKS - 1)

    def close(c, carry):
        first(0, c).wait_recv()
        second(c).wait_recv()
        rows = span(c, rows_chunk)
        value = partial[rows, cols(t)].astype(F32) + r1[0, c].astype(F32) + r2[c].astype(F32)
        out[rows, :] = (stream[rows, cols(t)].astype(F32) + value).astype(BF)
        first(0, c).wait_send()
        first(1, c).wait_send()
        second(c).wait_send()
        return carry

    lax.fori_loop(0, ROW_CHUNKS, close, 0)

    for c in range(SCAN_CHUNKS):
        e1_copy(c).wait_send()
        e2_copy(c).wait_send()

        @pl.when(z < m - 1)
        def _():
            chain_copy(c).wait_send()

    for c in range(ROW_CHUNKS):
        cross_copy(c).wait_send()
        stream_copy(c).wait_send()
    for kind in (0, 1):
        for dist in range(1, half_ring + 1):
            for is_first in (True, False) if dist < half_ring else (True,):
                for side in (0, 1):
                    hop_copy(kind, dist, is_first, side).wait_send()


def layer(n, *args):
    (residual, qw, kw, vw, dw, gw, qn, kn, vn, dn, gn, gain, outw, outn, mgain, up, down) = args
    tokens, wide = qw.shape
    keys = wide + qn.shape[1]
    values = vw.shape[1]
    width = outw.shape[1]
    inner = up.shape[1]
    own_width = width // 4
    block = min(128, tokens)
    blocks = tokens // block
    rc = tokens // ROW_CHUNKS
    hr = rc // 2
    anyspace = pl.BlockSpec(memory_space=pl.ANY)
    vspace = pl.BlockSpec(memory_space=VM)
    half = values // 2
    scratch = [
        VM((tokens, keys), BF), VM((tokens, keys), BF), VM((tokens, keys), BF),
        VM((tokens, values), BF), VM((tokens, values), BF),
        VM((tokens, values), BF), VM((tokens, values), BF),
        VM((2 * values, width), BF), VM((ROW_CHUNKS, hr, width), BF),
        VM(down.shape, BF), VM((2, n * up.shape[0], inner), BF),
        VM((tokens, keys), F32), VM((tokens, keys), BF), VM((blocks, values, keys), BF),
        VM((blocks, 1, keys), F32), VM((1, keys), F32), VM((values, keys), F32),
        VM((tokens, values), BF), VM((tokens, values), BF), VM((tokens, keys), BF),
        VM((16 + half, keys), BF), VM((16 + half, keys), BF),
        VM((half, keys), BF), VM((half, keys), BF), VM((half, keys), BF),
        VM((values, keys), BF),
        VM((rc, 2 * values), BF), VM((tokens, width), BF),
        VM((ROW_CHUNKS, hr, width), BF), VM((ROW_CHUNKS, hr, width), BF),
        VM((ROW_CHUNKS, hr, width), BF),
        VM((tokens, width), BF), VM((tokens, width), BF), VM((tokens, inner), BF),
        VM((2, ROW_CHUNKS, rc, own_width), BF), VM((ROW_CHUNKS, rc, own_width), BF),
        VM((ROW_CHUNKS, rc, own_width), BF),
        DMA((14 + ROW_CHUNKS,)),
        DMA((2, 2, n // 2, 2)), DMA((2, 2, n // 2, 2)),
    ] + [DMA((SCAN_CHUNKS,))] * 6 + [DMA((ROW_CHUNKS,))] * 6 + [
        DMA((2, ROW_CHUNKS)), DMA((2, ROW_CHUNKS)), DMA((ROW_CHUNKS,)), DMA((ROW_CHUNKS,)),
    ]
    in_specs = [anyspace] * 17
    in_specs[11] = in_specs[14] = vspace
    return pl.pallas_call(
        functools.partial(layer_kernel, n),
        out_shape=jax.ShapeDtypeStruct((tokens, own_width), BF),
        in_specs=in_specs,
        out_specs=vspace,
        scratch_shapes=scratch,
        compiler_params=pltpu.CompilerParams(
            collective_id=0, has_side_effects=True, vmem_limit_bytes=63 * 2**20
        ),
        cost_estimate=pl.CostEstimate(
            flops=30 * 10**9, bytes_accessed=32 * 2**20, transcendentals=0
        ),
        name="layer",
    )(*args)


def body(*args):
    n_sp, n_tp = lax.axis_size("sp"), lax.axis_size("tp")
    assert n_tp == HEADS == 4 and n_sp % 2 == 0
    args = list(args)
    args[11] = args[11].reshape(1, -1)
    args[14] = args[14].reshape(1, -1)
    return layer(n_sp, *args)


def solution(mesh):
    return jax.shard_map(
        body,
        mesh=mesh,
        in_specs=(
            P("sp", None),
            P("sp", "tp"),
            P("sp", "tp"),
            P("sp", "tp"),
            P("sp", "tp"),
            P("sp", "tp"),
            P("sp", "tp"),
            P("sp", "tp"),
            P("sp", "tp"),
            P("sp", "tp"),
            P("sp", "tp"),
            P(),
            P("tp", None),
            P("tp", None),
            P(),
            P("sp", "tp"),
            P("tp", "sp"),
        ),
        out_specs=P("sp", "tp"),
        check_vma=False,
    )
```

time: 204 us -> 135 us (0.66)
  Pallas kernels: 181 us -> 131 us
  between operations: 13.5 us -> 0.01 us
  local copies, waits for them, and re-layouts: 6.99 us -> 2.26 us
    pallas_call x5 -> x1, Pallas kernels: 181 us -> 131 us  [layer(): pl.pallas_call(functools.partial(layer_kernel, n), out_shape=jax.ShapeDty...]
    dynamic_slice x2 -> x0, local copies, waits for them, and re-layouts: 2.43 us -> none  [the longest x1 1.33 us: body(): lax.dynamic_slice_in_dim(residual, t * own_rows, own_rows, 0)]
    unnamed x19 -> x1, local copies, waits for them, and re-layouts: 4.56 us -> 2.26 us
  transfers between devices with their start and end apart: 1 -> 0, of which waited for: 0 -> 0; matrix products, arithmetic and copies ran while one was open for 1% -> 0% of each run, Pallas kernels for 71% -> 0%
where the time goes in v1:
time: 135 us; the launch traced here: 133 us
  Pallas kernels  131 us (97%)
  local copies, waits for them, and re-layouts  2.26 us (2%)
    pallas_call x1, Pallas kernels, layer(): pl.pallas_call(functools.partial(layer_kernel, n), out_shape=jax.ShapeDty...  131 us

profile of v1, /device:TPU:28, one launch (start us, length us, event | category | flops | bytes accessed | tf_op | source)
XLA Modules:
  0.0 133.3 jit_solution(17669840511880480074)
XLA Ops:
  0.0 131.0 %layer.1 = bf16[1024,512]{1,0:T(8,128)(2,1)} custom-call(bf16[1024,2048]{1,0:T(8,128)(2,1)} %residual.1, bf16[1024,256]{1,0:T(8,128)(2,1)} %qw.1, bf16[1024,256]{1,0:T(8,128)(2,1)} %kw.1, bf16[1024,512]{1,0:T(8,128)(2,1)} %vw.1, bf16[1024,256]{1,0:T(8,128)(2,1)} %dw.1, bf16[1024,512]{1,0:T(8,128)(2,1)} %gw.1, bf16[1024,128]{1,0:T(8,128)(2,1)} %qn.1, ...), custom_call_target="tpu_custom_call" | custom-call | flops 30000001024 | bytes 33554432 | tf_op jit(solution)/shard_map/layer/pallas_call | solution.py:508
  131.0 2.3 %copy.19 = bf16[1024,512]{1,0:T(8,128)(2,1)} copy(bf16[1024,512]{1,0:T(8,128)(2,1)} %layer.1) | data formatting | bytes 2097152

commit v2 on v1

--- a/solution.py
+++ b/solution.py
@@ -14,8 +14,9 @@
 F32 = jnp.float32
 VM = pltpu.VMEM
 DMA = pltpu.SemaphoreType.DMA
-SCAN_CHUNKS = 2
-ROW_CHUNKS = 4
+SCAN_CHUNKS = 4
+ROW_CHUNKS = 8
+EXPAND_CHUNKS = 4
 
 NT = ((1,), (1,))
 NN = ((1,), (0,))
@@ -27,7 +28,7 @@
 
 
 def span(i, size):
-    return pl.ds(pl.multiple_of(i * size, size), size)
+    return pl.ds(i * size if isinstance(i, int) else pl.multiple_of(i * size, size), size)
 
 
 def layer_kernel(
@@ -76,6 +77,9 @@
     for copy in loads:
         copy.start()
 
+    total[...] = jnp.zeros_like(total)
+    state[...] = jnp.zeros_like(state)
+
     place = jnp.where(y == 0, z, n - 1 - z)
 
     def index_of(p):
@@ -131,15 +135,13 @@
         jnp.int32, (block, block), 1
     )
     ones = tril.astype(F32).astype(BF)
-    total[...] = jnp.zeros_like(total)
-    state[...] = jnp.zeros_like(state)
     for copy in loads[1:7]:
         copy.wait()
 
     def pass_one(i, carry):
         rows = span(i, block)
         decay = d_all[rows, :].astype(F32)
-        g = (jnp.minimum(decay, 0.0) - jnp.log1p(jnp.exp(-jnp.abs(decay)))) / DECAY_NORMALIZER
+        g = (jnp.minimum(decay, 0.0) - jnp.log(1.0 + jnp.exp(-jnp.abs(decay)))) / DECAY_NORMALIZER
         high = g.astype(BF)
         low = (g - high.astype(F32)).astype(BF)
         within = dot(ones, high, NN) + dot(ones, low, NN)
@@ -198,18 +200,17 @@
     hop(0, 1, False, 0)
     loads[7].wait()
     weights[1, span(s, shard_rows), :] = d_shard[...].T
-    hop(1, 1, True, 1)
-    hop(1, 1, False, 1)
-    early_a = z >= 1
-    early_b = jnp.logical_and(z >= 2, z < m - 1)
+    inner_pair = z > 0
+    early_a = z >= 2
+
+    @pl.when(inner_pair)
+    def _():
+        hop(1, 1, True, 1)
+        hop(1, 1, False, 1)
 
     @pl.when(early_a)
     def _():
         hop(1, 1, True, 0)
-
-    @pl.when(early_b)
-    def _():
-        hop(1, 1, False, 0)
 
     for copy in loads[8:10]:
         copy.wait()
@@ -269,22 +270,24 @@
         e2s[where, :] = jnp.where(y == 0, between, before).astype(BF)
         e2_copy(c).start()
 
+    @pl.when(jnp.logical_not(inner_pair))
+    def _():
+        hop(1, 1, True, 1)
+        hop(1, 1, False, 1)
+
     @pl.when(jnp.logical_not(early_a))
     def _():
         hop(1, 1, True, 0)
 
-    @pl.when(jnp.logical_not(early_b))
-    def _():
-        hop(1, 1, False, 0)
+    hop(1, 1, False, 0)
 
     lax.fori_loop(ahead, blocks, pass_two, 0)
-    if half_ring >= 2:
-        hops(0, 2)
-        hops(1, 2)
     for copy in loads[10:]:
         copy.wait()
     for c in range(SCAN_CHUNKS):
         e2_copy(c).wait_recv()
+    if half_ring >= 2:
+        hops(0, 2)
 
     def near_copy(c):
         return pltpu.make_async_remote_copy(
@@ -367,85 +370,151 @@
     tile_h = min(512, inner)
 
     def expand(c, carry):
-        rows = span(c, rows_chunk)
+        rows = span(c, tokens // EXPAND_CHUNKS)
         for lo in range(0, inner, tile_h):
             h = dot(normed[rows, :], weights[0, :, lo : lo + tile_h], NN)
             hidden[rows, lo : lo + tile_h] = jnp.square(jnp.maximum(h, 0.0)).astype(BF)
         return carry
 
-    for dist in range(3, half_ring):
-        hops(0, dist)
-    settle(0)
-    settle(1)
-    if half_ring >= 3:
-        hops(0, half_ring)
-    for dist in range(3, half_ring):
-        hops(1, dist)
-    settle(2)
-    arrive(0)
-    lax.fori_loop(0, 3, expand, 0)
-    settle(3)
-    if half_ring >= 3:
-        hops(1, half_ring)
-    expand(3, 0)
-    arrive(1)
+    later = []
+    for dist in range(2, half_ring + 1):
+        group = [(1, dist, True), (0, dist + 1, True), (0, dist + 1, False), (1, dist, False)]
+        if dist > 2:
+            group[0], group[1] = group[1], group[0]
+        later += [h for h in group if h[1] < half_ring or (h[1] == half_ring and h[2])]
+    points = (0, 0, 2, 2, 4, 4, 6, ROW_CHUNKS + 1)
+    each = -(-len(later) // 6)
+    due = [points[i] if half_ring <= 4 else i // each for i in range(len(later))]
+
+    def serve(point):
+        for (kind, dist, is_first), at in zip(later, due):
+            if at == point:
+                for side in (0, 1):
+                    hop(kind, dist, is_first, side)
+
+    own_width = out.shape[1]
+    by_shard = shard_rows >= 128 and half_ring >= 3
+    shard = shard_rows if by_shard else max(shard_rows, 128)
+    shards = width // shard
+    per = own_width // shard
+    tall = tokens // 2
+    if by_shard:
+        near_by = 2 * (half_ring - 2) + 1
+        first_part = [near_by - 1, near_by - 2] + list(range(near_by - 2))
+        table = [(k, 0) for k in first_part]
+        table += [(near_by, 0), (near_by, 1), (first_part[0], 1), (first_part[1], 1)]
+        table += [(near_by + 1, 0), (near_by + 1, 1)] + [(k, 1) for k in first_part[2:]]
+        table += [(near_by + 2, 0), (near_by + 2, 1)]
+    else:
+        table = [(k, h) for h in (0, 1) for k in range(shards)]
+
+    def look(i, column):
+        value = table[0][column]
+        for n_row, row in enumerate(table[1:], 1):
+            value = jnp.where(i == n_row, row[column], value)
+        return value
+
+    def place_of(i):
+        k, h = look(i, 0), look(i, 1)
+        if by_shard:
+            dist = (k + 1) // 2
+            k = index_of(place + jnp.where(lax.rem(k, 2) == 1, dist, -dist))
+        return k, lax.rem(k, per), k // per, h
+
+    def to_near(which, q, j, h):
+        return pltpu.make_async_remote_copy(
+            src_ref=partial.at[span(h, tall), span(j, shard)],
+            dst_ref=r1.at[which, q, span(h, tall)],
+            send_sem=s1.at[which, q, h], recv_sem=v1.at[which, q, h],
+            device_id={"tp": near}, device_id_type=MESH,
+        )
+
+    def to_far(q, h):
+        return pltpu.make_async_remote_copy(
+            src_ref=mix.at[q, span(h, tall)], dst_ref=r2.at[q, span(h, tall)],
+            send_sem=s2.at[q, h], recv_sem=v2.at[q, h],
+            device_id={"tp": far}, device_id_type=MESH,
+        )
+
+    def across(i):
+        j, q, owner, h = place_of(i)
+
+        @pl.when(owner == far)
+        def _():
+            to_near(1, q, j, h).wait_recv()
+            rows = span(h, tall)
+            mix[q, rows] = (
+                partial[rows, span(j, shard)].astype(F32) + r1[1, q, rows].astype(F32)
+            ).astype(BF)
+            to_far(q, h).start()
+
+    def contract(begin, i, carry):
+        j, q, owner, h = place_of(i)
+        rows = span(h, tall)
+        partial[rows, span(j, shard)] = dot(
+            hidden[rows, :], weights[1, span(j, shard), :], NT
+        ).astype(BF)
+
+        @pl.when(owner == near)
+        def _():
+            to_near(0, q, j, h).start()
+
+        @pl.when(owner == cross)
+        def _():
+            to_near(1, q, j, h).start()
+
+        @pl.when(i > begin)
+        def _():
+            across(i - 1)
+
+        return carry
+
+    def contract_all(begin, end):
+        lax.fori_loop(begin, end, functools.partial(contract, begin), 0)
+        across(end - 1)
+
+    serve(0)
+    per_expand = ROW_CHUNKS // EXPAND_CHUNKS
     for c in range(ROW_CHUNKS):
-        near_copy(c).wait_send()
-
-    own_width = out.shape[1]
-
-    def cols(owner):
-        return span(owner, own_width)
-
-    def first(which, c):
-        return pltpu.make_async_remote_copy(
-            src_ref=partial.at[span(c, rows_chunk), cols((near, cross)[which])],
-            dst_ref=r1.at[which, c], send_sem=s1.at[which, c], recv_sem=v1.at[which, c],
-            device_id={"tp": near}, device_id_type=MESH,
-        )
-
-    def second(c):
-        return pltpu.make_async_remote_copy(
-            src_ref=mix.at[c], dst_ref=r2.at[c], send_sem=s2.at[c], recv_sem=v2.at[c],
-            device_id={"tp": far}, device_id_type=MESH,
-        )
-
-    def across(c):
-        first(1, c).wait_recv()
-        rows = span(c, rows_chunk)
-        mix[c] = (partial[rows, cols(far)].astype(F32) + r1[1, c].astype(F32)).astype(BF)
-        second(c).start()
-
-    def contract(c, carry):
-        rows = span(c, rows_chunk)
-        for lo in range(0, width, tile):
-            partial[rows, lo : lo + tile] = dot(
-                hidden[rows, :], weights[1, lo : lo + tile, :], NT
+        settle(c)
+        serve(c + 1)
+        if c == ROW_CHUNKS - per_expand - 1:
+            arrive(0)
+            lax.fori_loop(0, EXPAND_CHUNKS // 2, expand, 0)
+            for i in range(ROW_CHUNKS):
+                near_copy(i).wait_send()
+            if by_shard:
+                contract_all(0, near_by)
+            serve(ROW_CHUNKS + 1)
+            lax.fori_loop(EXPAND_CHUNKS // 2, EXPAND_CHUNKS - 1, expand, 0)
+    expand(EXPAND_CHUNKS - 1, 0)
+    if by_shard:
+        for side in (0, 1):
+            hop_copy(1, half_ring - 1, False, side).wait_recv()
+        contract_all(near_by, len(table) - 2)
+        for side in (0, 1):
+            hop_copy(1, half_ring, True, side).wait_recv()
+        contract_all(len(table) - 2, len(table))
+    else:
+        arrive(1)
+        contract_all(0, len(table))
+
+    for h in (0, 1):
+        for q in range(per):
+            j = t * per + q
+            rows = span(h, tall)
+            to_near(0, q, j, h).wait_recv()
+            to_far(q, h).wait_recv()
+            value = partial[rows, span(j, shard)].astype(F32) + r1[0, q, rows].astype(F32)
+            value = value + r2[q, rows].astype(F32)
+            out[rows, q * shard : (q + 1) * shard] = (
+                stream[rows, span(j, shard)].astype(F32) + value
             ).astype(BF)
-        first(1, c).start()
-        first(0, c).start()
-
-        @pl.when(c > 0)
-        def _():
-            across(c - 1)
-
-        return carry
-
-    lax.fori_loop(0, ROW_CHUNKS, contract, 0)
-    across(ROW_CHUNKS - 1)
-
-    def close(c, carry):
-        first(0, c).wait_recv()
-        second(c).wait_recv()
-        rows = span(c, rows_chunk)
-        value = partial[rows, cols(t)].astype(F32) + r1[0, c].astype(F32) + r2[c].astype(F32)
-        out[rows, :] = (stream[rows, cols(t)].astype(F32) + value).astype(BF)
-        first(0, c).wait_send()
-        first(1, c).wait_send()
-        second(c).wait_send()
-        return carry
-
-    lax.fori_loop(0, ROW_CHUNKS, close, 0)
+    for q in range(per):
+        for h in (0, 1):
+            to_near(0, q, near * per + q, h).wait_send()
+            to_near(1, q, cross * per + q, h).wait_send()
+            to_far(q, h).wait_send()
 
     for c in range(SCAN_CHUNKS):
         e1_copy(c).wait_send()
@@ -480,6 +549,8 @@
     anyspace = pl.BlockSpec(memory_space=pl.ANY)
     vspace = pl.BlockSpec(memory_space=VM)
     half = values // 2
+    shard = max(down.shape[1], 128)
+    per = own_width // shard
     scratch = [
         VM((tokens, keys), BF), VM((tokens, keys), BF), VM((tokens, keys), BF),
         VM((tokens, values), BF), VM((tokens, values), BF),
@@ -496,12 +567,12 @@
         VM((ROW_CHUNKS, hr, width), BF), VM((ROW_CHUNKS, hr, width), BF),
         VM((ROW_CHUNKS, hr, width), BF),
         VM((tokens, width), BF), VM((tokens, width), BF), VM((tokens, inner), BF),
-        VM((2, ROW_CHUNKS, rc, own_width), BF), VM((ROW_CHUNKS, rc, own_width), BF),
-        VM((ROW_CHUNKS, rc, own_width), BF),
+        VM((2, per, tokens, shard), BF), VM((per, tokens, shard), BF),
+        VM((per, tokens, shard), BF),
         DMA((14 + ROW_CHUNKS,)),
         DMA((2, 2, n // 2, 2)), DMA((2, 2, n // 2, 2)),
     ] + [DMA((SCAN_CHUNKS,))] * 6 + [DMA((ROW_CHUNKS,))] * 6 + [
-        DMA((2, ROW_CHUNKS)), DMA((2, ROW_CHUNKS)), DMA((ROW_CHUNKS,)), DMA((ROW_CHUNKS,)),
+        DMA((2, per, 2)), DMA((2, per, 2)), DMA((per, 2)), DMA((per, 2)),
     ]
     in_specs = [anyspace] * 17
     in_specs[11] = in_specs[14] = vspace

time: 135 us -> 116 us (0.86); the launches traced: 133 us -> 116 us
  Pallas kernels: 131 us -> 114 us
    pallas_call x1, Pallas kernels: 131 us -> 114 us  [layer(): pl.pallas_call(functools.partial(layer_kernel, n), out_shape=jax.ShapeDty...]
where the time goes in v2:
time: 116 us
  Pallas kernels  114 us (98%)
  local copies, waits for them, and re-layouts  2.26 us (2%)
    pallas_call x1, Pallas kernels, layer(): pl.pallas_call(functools.partial(layer_kernel, n), out_shape=jax.ShapeDty...  114 us

profile of v2, /device:TPU:28, one launch (start us, length us, event | category | flops | bytes accessed | tf_op | source)
XLA Modules:
  0.0 116.0 jit_solution(16152246099176112854)
XLA Ops:
  0.0 113.7 %layer.1 = bf16[1024,512]{1,0:T(8,128)(2,1)} custom-call(bf16[1024,2048]{1,0:T(8,128)(2,1)} %residual.1, bf16[1024,256]{1,0:T(8,128)(2,1)} %qw.1, bf16[1024,256]{1,0:T(8,128)(2,1)} %kw.1, bf16[1024,512]{1,0:T(8,128)(2,1)} %vw.1, bf16[1024,256]{1,0:T(8,128)(2,1)} %dw.1, bf16[1024,512]{1,0:T(8,128)(2,1)} %gw.1, bf16[1024,128]{1,0:T(8,128)(2,1)} %qn.1, ...), custom_call_target="tpu_custom_call" | custom-call | flops 30000001024 | bytes 33554432 | tf_op jit(solution)/shard_map/layer/pallas_call | solution.py:579
  113.7 2.3 %copy.19 = bf16[1024,512]{1,0:T(8,128)(2,1)} copy(bf16[1024,512]{1,0:T(8,128)(2,1)} %layer.1) | data formatting | bytes 2097152

commit v3 on v2

--- a/solution.py
+++ b/solution.py
@@ -14,9 +14,10 @@
 F32 = jnp.float32
 VM = pltpu.VMEM
 DMA = pltpu.SemaphoreType.DMA
-SCAN_CHUNKS = 4
+SCAN_CHUNKS = 8
 ROW_CHUNKS = 8
 EXPAND_CHUNKS = 4
+POINTS = (0, 0, 2, 4, 3, 5, 7, 9)
 
 NT = ((1,), (1,))
 NN = ((1,), (0,))
@@ -114,9 +115,9 @@
             hop_copy(kind, dist - 1, first, side).wait_recv()
         hop_copy(kind, dist, first, side).start()
 
-    def hops(kind, dist):
+    def hops(kind, dist, sides):
         for first in (True, False) if dist < half_ring else (True,):
-            for side in (0, 1):
+            for side in sides:
                 hop(kind, dist, first, side)
 
     def arrive(kind):
@@ -160,7 +161,7 @@
         total[...] = total[...] + last
         return carry
 
-    lax.fori_loop(0, blocks, pass_one, 0)
+    lax.fori_loop(0, blocks, pass_one, 0, unroll=2)
 
     half = values // 2
     part = half // SCAN_CHUNKS
@@ -275,19 +276,26 @@
         hop(1, 1, True, 1)
         hop(1, 1, False, 1)
 
-    @pl.when(jnp.logical_not(early_a))
-    def _():
-        hop(1, 1, True, 0)
-
-    hop(1, 1, False, 0)
+    def up_side():
+        if half_ring >= 2:
+            hops(0, 2, (0,))
+
+        @pl.when(jnp.logical_not(early_a))
+        def _():
+            hop(1, 1, True, 0)
+
+        hop(1, 1, False, 0)
+
+    pl.when(z < m - 1)(up_side)
+    if half_ring >= 2:
+        hops(0, 2, (1,))
 
     lax.fori_loop(ahead, blocks, pass_two, 0)
     for copy in loads[10:]:
         copy.wait()
     for c in range(SCAN_CHUNKS):
         e2_copy(c).wait_recv()
-    if half_ring >= 2:
-        hops(0, 2)
+    pl.when(z == m - 1)(up_side)
 
     def near_copy(c):
         return pltpu.make_async_remote_copy(
@@ -370,108 +378,125 @@
     tile_h = min(512, inner)
 
     def expand(c, carry):
-        rows = span(c, tokens // EXPAND_CHUNKS)
+        expand_rows(span(c, tokens // EXPAND_CHUNKS))
+        return carry
+
+    def expand_rows(rows):
         for lo in range(0, inner, tile_h):
             h = dot(normed[rows, :], weights[0, :, lo : lo + tile_h], NN)
             hidden[rows, lo : lo + tile_h] = jnp.square(jnp.maximum(h, 0.0)).astype(BF)
-        return carry
 
     later = []
     for dist in range(2, half_ring + 1):
-        group = [(1, dist, True), (0, dist + 1, True), (0, dist + 1, False), (1, dist, False)]
-        if dist > 2:
-            group[0], group[1] = group[1], group[0]
-        later += [h for h in group if h[1] < half_ring or (h[1] == half_ring and h[2])]
-    points = (0, 0, 2, 2, 4, 4, 6, ROW_CHUNKS + 1)
+        later += [(0, dist + 1, True), (0, dist + 1, False), (1, dist, True), (1, dist, False)]
+    later = [h for h in later if h[1] < half_ring or (h[1] == half_ring and h[2])]
+    points = POINTS
     each = -(-len(later) // 6)
-    due = [points[i] if half_ring <= 4 else i // each for i in range(len(later))]
+    due = [points[i] if half_ring == 4 else i // each for i in range(len(later))]
 
     def serve(point):
         for (kind, dist, is_first), at in zip(later, due):
             if at == point:
-                for side in (0, 1):
+                for side in (1, 0):
                     hop(kind, dist, is_first, side)
 
     own_width = out.shape[1]
-    by_shard = shard_rows >= 128 and half_ring >= 3
-    shard = shard_rows if by_shard else max(shard_rows, 128)
+    by_shard = shard_rows % 256 == 0 and half_ring >= 3
+    shard = max(shard_rows, 128)
     shards = width // shard
     per = own_width // shard
-    tall = tokens // 2
-    if by_shard:
-        near_by = 2 * (half_ring - 2) + 1
-        first_part = [near_by - 1, near_by - 2] + list(range(near_by - 2))
-        table = [(k, 0) for k in first_part]
-        table += [(near_by, 0), (near_by, 1), (first_part[0], 1), (first_part[1], 1)]
-        table += [(near_by + 1, 0), (near_by + 1, 1)] + [(k, 1) for k in first_part[2:]]
-        table += [(near_by + 2, 0), (near_by + 2, 1)]
-    else:
-        table = [(k, h) for h in (0, 1) for k in range(shards)]
-
-    def look(i, column):
-        value = table[0][column]
-        for n_row, row in enumerate(table[1:], 1):
-            value = jnp.where(i == n_row, row[column], value)
-        return value
-
-    def place_of(i):
-        k, h = look(i, 0), look(i, 1)
+    pieces = 2 if by_shard else 1
+    lanes = shard // pieces
+    row_parts = (pl.ds(0, tokens - rows_chunk), pl.ds(tokens - rows_chunk, rows_chunk))
+
+    def at_lane(i):
+        return pl.ds(i if isinstance(i, int) else pl.multiple_of(i, lanes), lanes)
+
+    def to_near(which, q, j, h, piece):
+        return pltpu.make_async_remote_copy(
+            src_ref=partial.at[row_parts[h], at_lane(j * shard + piece * lanes)],
+            dst_ref=r1.at[which, q, row_parts[h], at_lane(piece * lanes)],
+            send_sem=s1.at[which, q, h, piece], recv_sem=v1.at[which, q, h, piece],
+            device_id={"tp": near}, device_id_type=MESH,
+        )
+
+    def to_far(q, h, piece):
+        where = (q, row_parts[h], at_lane(piece * lanes))
+        return pltpu.make_async_remote_copy(
+            src_ref=mix.at[where], dst_ref=r2.at[where],
+            send_sem=s2.at[q, h, piece], recv_sem=v2.at[q, h, piece],
+            device_id={"tp": far}, device_id_type=MESH,
+        )
+
+    def place_of(k):
         if by_shard:
             dist = (k + 1) // 2
             k = index_of(place + jnp.where(lax.rem(k, 2) == 1, dist, -dist))
-        return k, lax.rem(k, per), k // per, h
-
-    def to_near(which, q, j, h):
-        return pltpu.make_async_remote_copy(
-            src_ref=partial.at[span(h, tall), span(j, shard)],
-            dst_ref=r1.at[which, q, span(h, tall)],
-            send_sem=s1.at[which, q, h], recv_sem=v1.at[which, q, h],
-            device_id={"tp": near}, device_id_type=MESH,
-        )
-
-    def to_far(q, h):
-        return pltpu.make_async_remote_copy(
-            src_ref=mix.at[q, span(h, tall)], dst_ref=r2.at[q, span(h, tall)],
-            send_sem=s2.at[q, h], recv_sem=v2.at[q, h],
-            device_id={"tp": far}, device_id_type=MESH,
-        )
-
-    def across(i):
-        j, q, owner, h = place_of(i)
+        return k, lax.rem(k, per), k // per
+
+    def pieces_of(k, part):
+        if part is None:
+            return list(range(pieces))
+        return [lax.rem(k, 2) if part == 0 else 1 - lax.rem(k, 2)]
+
+    def across(k, h, part):
+        j, q, owner = place_of(k)
 
         @pl.when(owner == far)
         def _():
-            to_near(1, q, j, h).wait_recv()
-            rows = span(h, tall)
-            mix[q, rows] = (
-                partial[rows, span(j, shard)].astype(F32) + r1[1, q, rows].astype(F32)
-            ).astype(BF)
-            to_far(q, h).start()
-
-    def contract(begin, i, carry):
-        j, q, owner, h = place_of(i)
-        rows = span(h, tall)
-        partial[rows, span(j, shard)] = dot(
-            hidden[rows, :], weights[1, span(j, shard), :], NT
+            for piece in pieces_of(k, part):
+                to_near(1, q, j, h, piece).wait_recv()
+                here = (q, row_parts[h], at_lane(piece * lanes))
+                mine = partial[row_parts[h], at_lane(j * shard + piece * lanes)]
+                mix[here] = (mine.astype(F32) + r1[(1,) + here].astype(F32)).astype(BF)
+                to_far(q, h, piece).start()
+
+    def contract(k, h, part):
+        j, q, owner = place_of(k)
+        which = pieces_of(k, part)
+        size = shard if part is None else lanes
+        start = pl.multiple_of(j * shard + (0 if part is None else which[0] * lanes), lanes)
+        columns = pl.ds(start, size)
+        partial[row_parts[h], columns] = dot(
+            hidden[row_parts[h], :], weights[1, columns, :], NT
         ).astype(BF)
 
         @pl.when(owner == near)
         def _():
-            to_near(0, q, j, h).start()
+            for piece in which:
+                to_near(0, q, j, h, piece).start()
 
         @pl.when(owner == cross)
         def _():
-            to_near(1, q, j, h).start()
-
-        @pl.when(i > begin)
-        def _():
-            across(i - 1)
-
-        return carry
-
-    def contract_all(begin, end):
-        lax.fori_loop(begin, end, functools.partial(contract, begin), 0)
-        across(end - 1)
+            for piece in which:
+                to_near(1, q, j, h, piece).start()
+
+    pending = []
+
+    def flush():
+        while pending:
+            across(*pending.pop())
+
+    def run(order, h, part=None):
+        def look(i):
+            value = order[0]
+            for n_row, k in enumerate(order[1:], 1):
+                value = jnp.where(i == n_row, k, value)
+            return value
+
+        def step(i, carry):
+            contract(look(i), h, part)
+            if pending:
+                pl.when(i == 0)(lambda: across(*pending[0]))
+            pl.when(i > 0)(lambda: across(look(i - 1), h, part))
+            return carry
+
+        lax.fori_loop(0, len(order), step, 0)
+        pending[:] = [(jnp.int32(order[-1]), h, part)]
+
+    near_by = 2 * (half_ring - 2) + 1
+    close_order = [near_by - 1, near_by - 2] + list(range(near_by - 2))
+    third = [near_by, near_by + 1]
 
     serve(0)
     per_expand = ROW_CHUNKS // EXPAND_CHUNKS
@@ -480,41 +505,32 @@
         serve(c + 1)
         if c == ROW_CHUNKS - per_expand - 1:
             arrive(0)
-            lax.fori_loop(0, EXPAND_CHUNKS // 2, expand, 0)
+            lax.fori_loop(0, EXPAND_CHUNKS - 1, expand, 0)
             for i in range(ROW_CHUNKS):
                 near_copy(i).wait_send()
-            if by_shard:
-                contract_all(0, near_by)
+        if c >= ROW_CHUNKS - per_expand:
+            expand_rows(span(c, rows_chunk))
+        if c == ROW_CHUNKS - 2 and by_shard:
+            run(close_order, 0)
             serve(ROW_CHUNKS + 1)
-            lax.fori_loop(EXPAND_CHUNKS // 2, EXPAND_CHUNKS - 1, expand, 0)
-    expand(EXPAND_CHUNKS - 1, 0)
+            run(third, 0, 0)
+            flush()
     if by_shard:
+        run(close_order, 1)
+        run(third, 1, 0)
         for side in (0, 1):
             hop_copy(1, half_ring - 1, False, side).wait_recv()
-        contract_all(near_by, len(table) - 2)
+        run(third, 0, 1)
+        run(third, 1, 1)
         for side in (0, 1):
             hop_copy(1, half_ring, True, side).wait_recv()
-        contract_all(len(table) - 2, len(table))
+        run([shards - 1], 0)
+        run([shards - 1], 1)
     else:
         arrive(1)
-        contract_all(0, len(table))
-
-    for h in (0, 1):
-        for q in range(per):
-            j = t * per + q
-            rows = span(h, tall)
-            to_near(0, q, j, h).wait_recv()
-            to_far(q, h).wait_recv()
-            value = partial[rows, span(j, shard)].astype(F32) + r1[0, q, rows].astype(F32)
-            value = value + r2[q, rows].astype(F32)
-            out[rows, q * shard : (q + 1) * shard] = (
-                stream[rows, span(j, shard)].astype(F32) + value
-            ).astype(BF)
-    for q in range(per):
         for h in (0, 1):
-            to_near(0, q, near * per + q, h).wait_send()
-            to_near(1, q, cross * per + q, h).wait_send()
-            to_far(q, h).wait_send()
+            run(list(range(shards)), h)
+    flush()
 
     for c in range(SCAN_CHUNKS):
         e1_copy(c).wait_send()
@@ -532,6 +548,32 @@
             for is_first in (True, False) if dist < half_ring else (True,):
                 for side in (0, 1):
                     hop_copy(kind, dist, is_first, side).wait_send()
+
+    for q in range(per):
+        for h in (0, 1):
+            for piece in range(pieces):
+                to_near(0, q, near * per + q, h, piece).wait_send()
+                to_near(1, q, cross * per + q, h, piece).wait_send()
+
+    for h in (0, 1):
+        for q in range(per):
+            for piece in range(pieces):
+                j = t * per + q
+                rows = row_parts[h]
+                to_near(0, q, j, h, piece).wait_recv()
+                to_far(q, h, piece).wait_recv()
+                columns = at_lane(j * shard + piece * lanes)
+                inside = at_lane(piece * lanes)
+                value = partial[rows, columns].astype(F32) + r1[0, q, rows, inside].astype(F32)
+                value = value + r2[q, rows, inside].astype(F32)
+                lo = q * shard + piece * lanes
+                out[rows, lo : lo + lanes] = (
+                    stream[rows, columns].astype(F32) + value
+                ).astype(BF)
+    for q in range(per):
+        for h in (0, 1):
+            for piece in range(pieces):
+                to_far(q, h, piece).wait_send()
 
 
 def layer(n, *args):
@@ -572,18 +614,18 @@
         DMA((14 + ROW_CHUNKS,)),
         DMA((2, 2, n // 2, 2)), DMA((2, 2, n // 2, 2)),
     ] + [DMA((SCAN_CHUNKS,))] * 6 + [DMA((ROW_CHUNKS,))] * 6 + [
-        DMA((2, per, 2)), DMA((2, per, 2)), DMA((per, 2)), DMA((per, 2)),
+        DMA((2, per, 2, 2)), DMA((2, per, 2, 2)), DMA((per, 2, 2)), DMA((per, 2, 2)),
     ]
     in_specs = [anyspace] * 17
     in_specs[11] = in_specs[14] = vspace
     return pl.pallas_call(
         functools.partial(layer_kernel, n),
-        out_shape=jax.ShapeDtypeStruct((tokens, own_width), BF),
+        out_shape=VM((tokens, own_width), BF),
         in_specs=in_specs,
         out_specs=vspace,
         scratch_shapes=scratch,
         compiler_params=pltpu.CompilerParams(
-            collective_id=0, has_side_effects=True, vmem_limit_bytes=63 * 2**20
+            collective_id=0, has_side_effects=True, vmem_limit_bytes=60 * 2**20
         ),
         cost_estimate=pl.CostEstimate(
             flops=30 * 10**9, bytes_accessed=32 * 2**20, transcendentals=0

time: 116 us -> 110 us (0.948)
  Pallas kernels: 114 us -> 109 us
  local copies, waits for them, and re-layouts: 2.26 us -> 0.97 us
    pallas_call x1, Pallas kernels: 114 us -> 109 us  [layer(): pl.pallas_call(functools.partial(layer_kernel, n), out_shape=VM((tokens,...]
    unnamed x1, local copies, waits for them, and re-layouts: 2.26 us -> 0.97 us
where the time goes in v3:
time: 110 us
  Pallas kernels  109 us (99%)
    pallas_call x1, Pallas kernels, layer(): pl.pallas_call(functools.partial(layer_kernel, n), out_shape=VM((tokens,...  109 us

profile of v3, /device:TPU:28, one launch (start us, length us, event | category | flops | bytes accessed | tf_op | source)
XLA Modules:
  0.0 109.6 jit_solution(3921761822749745679)
XLA Ops:
  0.0 108.6 %layer.1 = bf16[1024,512]{1,0:T(8,128)(2,1)S(1)} custom-call(bf16[1024,2048]{1,0:T(8,128)(2,1)} %residual.1, bf16[1024,256]{1,0:T(8,128)(2,1)} %qw.1, bf16[1024,256]{1,0:T(8,128)(2,1)} %kw.1, bf16[1024,512]{1,0:T(8,128)(2,1)} %vw.1, bf16[1024,256]{1,0:T(8,128)(2,1)} %dw.1, bf16[1024,512]{1,0:T(8,128)(2,1)} %gw.1, bf16[1024,128]{1,0:T(8,128)(2,1)} %qn.1, ...), custom_call_target="tpu_custom_call" | custom-call | flops 30000001024 | bytes 33554432 | tf_op jit(solution)/shard_map/layer/pallas_call | solution.py:621
  108.6 1.0 copy.19

commit v4 on v3

--- a/solution.py
+++ b/solution.py
@@ -17,7 +17,7 @@
 SCAN_CHUNKS = 8
 ROW_CHUNKS = 8
 EXPAND_CHUNKS = 4
-POINTS = (0, 0, 2, 4, 3, 5, 7, 9)
+POINTS = (0, 0, 3, 4, 2, 6, 7, 9)
 
 NT = ((1,), (1,))
 NN = ((1,), (0,))
@@ -294,8 +294,9 @@
     for copy in loads[10:]:
         copy.wait()
     for c in range(SCAN_CHUNKS):
+        if c == SCAN_CHUNKS // 2 + 1:
+            pl.when(z == m - 1)(up_side)
         e2_copy(c).wait_recv()
-    pl.when(z == m - 1)(up_side)
 
     def near_copy(c):
         return pltpu.make_async_remote_copy(

time: 110 us -> 109 us (level)
  Pallas kernels: 109 us -> 107 us
    pallas_call x1, Pallas kernels: 109 us -> 107 us  [layer(): pl.pallas_call(functools.partial(layer_kernel, n), out_shape=VM((tokens,...]
where the time goes in v4:
time: 109 us; the launch traced here: 108 us
  Pallas kernels  107 us (98%)
    pallas_call x1, Pallas kernels, layer(): pl.pallas_call(functools.partial(layer_kernel, n), out_shape=VM((tokens,...  107 us

profile of v4, /device:TPU:28, one launch (start us, length us, event | category | flops | bytes accessed | tf_op | source)
XLA Modules:
  0.0 108.5 jit_solution(11108706248480389887)
XLA Ops:
  0.0 107.5 %layer.1 = bf16[1024,512]{1,0:T(8,128)(2,1)S(1)} custom-call(bf16[1024,2048]{1,0:T(8,128)(2,1)} %residual.1, bf16[1024,256]{1,0:T(8,128)(2,1)} %qw.1, bf16[1024,256]{1,0:T(8,128)(2,1)} %kw.1, bf16[1024,512]{1,0:T(8,128)(2,1)} %vw.1, bf16[1024,256]{1,0:T(8,128)(2,1)} %dw.1, bf16[1024,512]{1,0:T(8,128)(2,1)} %gw.1, bf16[1024,128]{1,0:T(8,128)(2,1)} %qn.1, ...), custom_call_target="tpu_custom_call" | custom-call | flops 30000001024 | bytes 33554432 | tf_op jit(solution)/shard_map/layer/pallas_call | solution.py:622
  107.5 1.0 copy.19
